TPU v7x, 32 devices: a whole 2x2x4 slice. The times are simulated.
32 devices in a mesh: sp: 8 (over z, core), tp: 4 (over y, x).
Axes of the slice: x: 2, y: 2, z: 4, core: 2. Of those that a mesh axis runs over, the one named last changes fastest.
Arguments:
- residual: bfloat16 [1024, 4096], P('sp', 'tp'), may hold values from -46 to 46
- query_small: bfloat16 [1024, 2048], P('sp', 'tp'), may hold values from -6 to 6
- key_narrow_group: bfloat16 [1024, 2048], P('sp', 'tp'), may hold values from -6 to 6
- query_large: bfloat16 [1024, 4096], P('sp', 'tp'), may hold values from -6 to 6
- key_large: bfloat16 [1024, 4096], P('sp', 'tp'), may hold values from -6 to 6
- values: bfloat16 [1024, 2, 2048], P('sp', None, 'tp'), may hold values from -6 to 6
- gates: bfloat16 [1024, 2, 2048], P('sp', None, 'tp'), may hold values from -6 to 6
- log_decay: float32 [1024, 2, 16], P('sp', None, 'tp'), may hold values from -0.65 to 0, as said below
- head_gain: float32 [2, 2048], P(None, 'tp'), may hold values from 0.1 to 1.9
- out_weight: bfloat16 [2, 2048, 4096], P(None, 'sp', 'tp'), may hold values from -0.09375 to 0.09375
- norm_gain: float32 [4096], P('tp'), may hold values from 0.1 to 1.9
- routes: int32 [1024, 2], P('sp'), may hold values from 0 to 7, all different within a row; in each aligned block of 128 rows (0 to 127, 128 to 255, ...) at most 64 rows name the same one
- route_weight: float32 [1024, 2], P('sp'), may hold values from 0.2 to 1
- expert_gate: bfloat16 [8, 4096, 2048], P('sp', None, 'tp'), may hold values from -0.09375 to 0.09375
- expert_up: bfloat16 [8, 4096, 2048], P('sp', None, 'tp'), may hold values from -0.09375 to 0.09375
- expert_down: bfloat16 [8, 2048, 4096], P('sp', None, 'tp'), may hold values from -0.5 to 0.5
Outputs:
- new_stream: bfloat16 [1024, 4096], P('sp', 'tp')
Inputs may be any that keep to these rules, and one draw needn't show every extreme that they name: `routes`: each row names two different experts; in each aligned block of 128 rows no expert is named more than 64 times, a bound that some block reaches. `log_decay`: negative at every position.
All inputs are finite; a program needn't handle non-finite values.
Results may differ from a plain program's by a relative error of at most 0.019.
Values may be sent and summed in bfloat16 or wider, within the bound.
No kernel may reach another device: no remote copies, remote signals or barrier semaphores. Data moves between devices by JAX's collectives and lax.ppermute only.
A program may use at most 64 MiB of HBM per device.

v0:
```python
import jax
import jax.numpy as jnp
from jax import lax
from jax.sharding import PartitionSpec as P

D = 4096
EPS = 1e-06
THETA = 10000.0


def entering_2(array, axis, combine, identity):
    devices, place = (lax.axis_size(axis), lax.axis_index(axis))
    everything = jax.tree.map(lambda part: lax.all_gather(part, axis), array)
    start = jax.tree.map(
        lambda part, zero: jnp.broadcast_to(jnp.asarray(zero, part.dtype), part.shape),
        array,
        identity,
    )

    def step(k, before):
        reached = k < place
        new = combine(before, jax.tree.map(lambda part: part[k], everything))
        return jax.tree.map(lambda a, b: jnp.where(reached, a, b), new, before)

    return lax.fori_loop(0, devices, step, start)


def rotate(block, positions):
    half_dim = block.shape[-1] // 2
    inverse = jnp.power(THETA, -jnp.arange(half_dim, dtype=jnp.float32) * 2.0 / block.shape[-1])
    angles = positions[:, None, None] * inverse
    cosine_val, sine_val = (jnp.cos(angles), jnp.sin(angles))
    lower_half, upper_half = (block[..., :half_dim], block[..., half_dim:])
    return jnp.concatenate(
        [
            lower_half * cosine_val - upper_half * sine_val,
            upper_half * cosine_val + lower_half * sine_val,
        ],
        axis=-1,
    )


def block_terms(rot_queries, rot_keys, value_heads, rates):
    count = rates.shape[0]
    decay_sum = jnp.cumsum(rates, axis=0)
    by_head = decay_sum.T
    causal = (jnp.arange(count)[:, None] >= jnp.arange(count)[None, :])[None]
    spread = by_head[:, :, None] - by_head[:, None, :]
    weight = jnp.where(causal, jnp.exp(jnp.where(causal, spread, 0.0)), 0.0)
    scores = jnp.einsum("ihd,jhd->hij", rot_queries, rot_keys, preferred_element_type=jnp.float32)
    weighted = (scores * weight).astype(jnp.bfloat16)
    within = jnp.einsum("hij,jhv->ihv", weighted, value_heads, preferred_element_type=jnp.float32)
    block_end = decay_sum[-1]
    carried = (
        rot_keys.astype(jnp.float32) * jnp.exp(block_end[None, :] - decay_sum)[:, :, None]
    ).astype(jnp.bfloat16)
    update = jnp.einsum("jhd,jhv->hdv", carried, value_heads, preferred_element_type=jnp.float32)
    return (within, decay_sum, jnp.exp(block_end), update)


def final_result(rot_queries, decay_sum, within, state_in, gate_part, gain_part):
    cross_part = (
        jnp.einsum(
            "ihd,hdv->ihv",
            rot_queries.astype(jnp.float32),
            state_in,
            precision=lax.Precision.HIGHEST,
        )
        * jnp.exp(decay_sum)[:, :, None]
    )
    retained = within + cross_part
    scaled = retained * lax.rsqrt(jnp.mean(retained * retained, axis=-1, keepdims=True) + EPS)
    count, head_count, value_size = retained.shape
    gated = jax.nn.silu(gate_part.astype(jnp.float32)).reshape(count, head_count, value_size)
    return (
        (scaled * gain_part.reshape(head_count, value_size) * gated)
        .reshape(count, -1)
        .astype(jnp.bfloat16)
    )


def prepare(queries, keys_in, value_part, positions, head_count):
    row_count = queries.shape[0]
    key_size = queries.shape[1] // head_count
    rot_queries = rotate(
        queries.astype(jnp.float32).reshape(row_count, head_count, key_size), positions
    ).astype(jnp.bfloat16)
    rot_keys = (
        rotate(keys_in.astype(jnp.float32).reshape(row_count, head_count, key_size), positions)
        * key_size ** (-0.5)
    ).astype(jnp.bfloat16)
    value_heads = value_part.reshape(row_count, head_count, value_part.shape[1] // head_count)
    return (rot_queries, rot_keys, value_heads)


def per_device(
    residual,
    query_small,
    key_narrow_group,
    query_large,
    key_large,
    values,
    gates,
    log_decay,
    head_gain,
    out_weight,
    norm_gain,
    routes,
    route_weight,
    expert_gate,
    expert_up,
    expert_down,
):
    row_count = residual.shape[0]
    head_count = log_decay.shape[2]
    positions = (lax.axis_index("sp") * row_count + jnp.arange(row_count, dtype=jnp.int32)).astype(
        jnp.float32
    )
    query_a, key_a, value_a = prepare(
        query_small, key_narrow_group, values[:, 0], positions, head_count
    )
    query_b, key_b, value_b = prepare(query_large, key_large, values[:, 1], positions, head_count)
    within_a, decay_sum_a, fall_a, update_a = block_terms(query_a, key_a, value_a, log_decay[:, 0])
    within_b, decay_sum_b, fall_b, update_b = block_terms(query_b, key_b, value_b, log_decay[:, 1])

    def combine(before_part, after_part):
        return (
            before_part[0] * after_part[0],
            after_part[0][:, None, None] * before_part[1] + after_part[1],
            before_part[2] * after_part[2],
            after_part[2][:, None, None] * before_part[3] + after_part[3],
        )

    identity = (
        jnp.ones_like(fall_a),
        jnp.zeros_like(update_a),
        jnp.ones_like(fall_b),
        jnp.zeros_like(update_b),
    )
    entering = entering_2((fall_a, update_a, fall_b, update_b), "sp", combine, identity)
    output_a = final_result(query_a, decay_sum_a, within_a, entering[1], gates[:, 0], head_gain[0])
    output_b = final_result(query_b, decay_sum_b, within_b, entering[3], gates[:, 1], head_gain[1])
    stacked = jnp.stack([output_a, output_b], axis=1)
    gathered = lax.all_gather(stacked, "tp", axis=2, tiled=True)
    mixed = jnp.einsum(
        "tgk,gkd->td",
        gathered,
        lax.all_gather(out_weight, "sp", axis=1, tiled=True),
        preferred_element_type=jnp.float32,
    ).astype(jnp.bfloat16)
    stream = residual.astype(jnp.float32) + mixed.astype(jnp.float32)
    square_sum = lax.psum(jnp.sum(stream * stream, axis=1), "tp")
    normed = (stream * lax.rsqrt(square_sum / D + EPS)[:, None] * norm_gain[None, :]).astype(
        jnp.bfloat16
    )
    experts = lax.axis_size("sp")
    capacity = 4 * row_count // experts
    one_hot = (routes[:, :, None] == jnp.arange(experts, dtype=jnp.int32)[None, None, :]).astype(
        jnp.int32
    )
    one_hot = one_hot.reshape(2 * row_count, experts)
    before = jnp.cumsum(one_hot, axis=0) - one_hot
    slot_index = jnp.sum(before * one_hot, axis=1).reshape(row_count, 2)
    target = routes * capacity + slot_index
    slot_ids = jnp.arange(experts * capacity, dtype=jnp.int32)
    choose = target[:, :, None] == slot_ids[None, None, :]
    select = jnp.sum(choose.astype(jnp.int32), axis=1).astype(jnp.bfloat16).T
    w_gate, w_up, w_down = (expert_gate[0], expert_up[0], expert_down[0])
    outgoing = jnp.dot(select, normed, preferred_element_type=jnp.float32).astype(jnp.bfloat16)
    outgoing = outgoing.reshape(experts, capacity, normed.shape[1])
    arrived = lax.all_to_all(outgoing, "sp", split_axis=0, concat_axis=0, tiled=True)
    expert_arrived = lax.all_gather(arrived, "tp", axis=2, tiled=True)
    gate_part = jnp.einsum(
        "sck,kf->scf", expert_arrived, w_gate, preferred_element_type=jnp.float32
    )
    up_part = jnp.einsum("sck,kf->scf", expert_arrived, w_up, preferred_element_type=jnp.float32)
    hidden = (jax.nn.silu(gate_part) * up_part).astype(jnp.bfloat16)
    expert_out = jnp.einsum(
        "scf,fd->scd",
        lax.all_gather(hidden, "tp", axis=2, tiled=True),
        w_down,
        preferred_element_type=jnp.float32,
    ).astype(jnp.bfloat16)
    returned = lax.all_to_all(expert_out, "sp", split_axis=0, concat_axis=0, tiled=True).reshape(
        experts * capacity, -1
    )
    first_pick = jnp.dot(
        choose[:, 0].astype(jnp.bfloat16), returned, preferred_element_type=jnp.float32
    )
    second_pick = jnp.dot(
        choose[:, 1].astype(jnp.bfloat16), returned, preferred_element_type=jnp.float32
    )
    routed = route_weight[:, 0:1] * first_pick + route_weight[:, 1:2] * second_pick
    return (stream + routed).astype(jnp.bfloat16)


def solution(mesh):
    placed = (
        P("sp", "tp"),
        P("sp", "tp"),
        P("sp", "tp"),
        P("sp", "tp"),
        P("sp", "tp"),
        P("sp", None, "tp"),
        P("sp", None, "tp"),
        P("sp", None, "tp"),
        P(None, "tp"),
        P(None, "sp", "tp"),
        P("tp"),
        P("sp", None),
        P("sp", None),
        P("sp", None, "tp"),
        P("sp", None, "tp"),
        P("sp", None, "tp"),
    )
    return jax.shard_map(
        per_device, mesh=mesh, in_specs=placed, out_specs=P("sp", "tp"), check_vma=False
    )
```

profile of v0, /device:TPU:0, one launch (start us, length us, event | category | flops | bytes accessed | tf_op | source)
XLA Modules:
  0.0 408.3 jit_solution(11339238263994428955)
XLA Ops:
  6.6 0.7 slice_bitcast_fusion.4
  7.3 1.5 fusion.79
  8.8 1.0 copy.129
  10.1 1.0 copy.132
  12.7 1.0 fusion.45
  15.9 1.2 fusion.32
  18.2 13.6 %all-gather.3 = f32[8,1,4]{2,1,0:T(1,128)S(1)} all-gather(f32[1,1,4]{2,1,0:T(1,128)S(1)} %get-tuple-element.253), channel_id=1, replica_groups=mesh['sp'=8,'tp'=4] {'sp'}, dimensions={0}, use_global_device_ids=true | all-gather | bytes 144 | tf_op jit(solution)/shard_map/all_gather | solution.py:13
  31.8 9.0 %all-gather.2 = f32[8,1,4]{2,1,0:T(1,128)S(1)} all-gather(f32[1,1,4]{2,1,0:T(1,128)S(1)} %get-tuple-element.255), channel_id=1, replica_groups=mesh['sp'=8,'tp'=4] {'sp'}, dimensions={0}, use_global_device_ids=true | all-gather | bytes 144 | tf_op jit(solution)/shard_map/all_gather | solution.py:13
  40.8 0.4 convolution_bitcast_fusion.4
  41.3 4.5 %all-gather.19.cloned.1.call-done = f32[32,128,128]{2,1,0:T(8,128)} async-done(((f32[4,128,128]{2,1,0:T(8,128)}), f32[32,128,128]{2,1,0:T(8,128)}) %all-gather.19.cloned.1.call-update) | async-done | bytes 2097168 | tf_op jit(solution)/shard_map/all_gather | solution.py:13
  45.8 47.9 %all-gather.21.cloned.1.call-done = f32[32,256,128]{2,1,0:T(8,128)} async-done(((f32[4,256,128]{2,1,0:T(8,128)}), f32[32,256,128]{2,1,0:T(8,128)}) %all-gather.21.cloned.1.call-update) | async-done | bytes 4194320 | tf_op jit(solution)/shard_map/all_gather | solution.py:13
  93.7 18.1 %while.16 = (s32[]{:T(128)}, f32[4,128,128]{2,1,0:T(8,128)S(1)}, f32[4,256,128]{2,1,0:T(8,128)S(1)}, s32[]{:T(128)}, f32[8,4]{1,0:T(8,128)S(1)}, /*index=5*/f32[...) while((s32[]{:T(128)}, f32[4,128,128]{2,1,0:T(8,128)S(1)}, ...), condition=%wide.region_3.4_spmd.clone, body=%wide.region_2.3_spmd.clone.sunk | while | flops 786436 | bytes 2359527 | solution.py:25
  93.7 1.2 fusion.106
  94.9 1.1 fusion.105
  96.0 1.2 fusion.106
  97.2 1.1 fusion.105
  98.2 1.2 fusion.106
  99.4 1.1 fusion.105
  100.5 1.2 fusion.106
  101.7 1.1 fusion.105
  102.8 1.2 fusion.106
  104.0 1.1 fusion.105
  105.1 1.2 fusion.106
  106.2 1.1 fusion.105
  107.3 1.2 fusion.106
  108.5 1.1 fusion.105
  109.6 1.2 fusion.106
  110.8 1.1 fusion.105
  111.9 0.5 multiply_reduce_fusion.2
  112.6 0.6 fusion.25
  113.3 0.4 multiply_reduce_fusion.1
  113.9 0.7 pad_maximum_fusion.1
  114.7 0.5 all-gather.13.cloned.1.call-update
  115.7 0.6 reduce-window.6
  117.0 23.0 %all-gather.11.cloned.1.call-done = bf16[128,2,2048]{2,0,1:T(8,128)(2,1)} async-done(((bf16[128,2,512]{2,0,1:T(8,128)(2,1)}), bf16[128,2,2048]{2,0,1:T(8,128)(2,1)}) %all-gather.11.cloned.1.call-update) | async-done | bytes 1048592 | tf_op jit(solution)/shard_map/all_gather | solution.py:144
  140.0 83.5 %all-gather.13.cloned.1.call-done = bf16[2,2048,1024]{2,1,0:T(8,128)(2,1)} async-done(((bf16[2,256,1024]{2,1,0:T(8,128)(2,1)}), bf16[2,2048,1024]{2,1,0:T(8,128)(2,1)}) %all-gather.13.cloned.1.call-update) | async-done | bytes 8388624 | tf_op jit(solution)/shard_map/all_gather | solution.py:148
  223.6 5.1 %multiply_reduce_fusion = (f32[128]{0:T(128)S(1)}, f32[128,1024]{1,0:T(8,128)S(1)}) fusion(bf16[128,2,2048]{2,0,1:T(8,128)(2,1)} %all-gather.11.cloned.1.call-done, bf16[2,2048,1024]{2,1,0:T(8,128)(2,1)} %all-gather.13.cloned.1.call-done, bf16[128,1024]{1,0:T(8,128)(2,1)S(1)} %copy-done.1), kind=kOutput, calls=%fused_computation.42 | convolution fusion | flops 1074528128 | bytes 10224128 | tf_op jit(solution)/shard_map/tgk,gkd->td/dot_general | solution.py:145
  228.6 9.8 %psum.7 = f32[128]{0:T(128)S(1)} all-reduce(f32[128]{0:T(128)S(1)} %get-tuple-element.270), channel_id=1, replica_groups=mesh['sp'=8,'tp'=4] {'tp'}, use_global_device_ids=true, to_apply=%region_11.12 | all-reduce | flops 128 | bytes 1024 | tf_op jit(solution)/shard_map/psum | solution.py:152
  238.5 0.5 convolution_convert_fusion
  239.0 29.7 %all_to_all.10 = bf16[8,64,1024]{2,1,0:T(8,128)(2,1)} all-to-all(bf16[8,64,1024]{2,1,0:T(8,128)(2,1)S(1)} %bitcast.130), channel_id=1, replica_groups=mesh['sp'=8,'tp'=4] {'sp'}, dimensions={0} | all-to-all | bytes 2097152 | tf_op jit(solution)/shard_map/all_to_all | solution.py:171
  268.9 49.5 %all-gather.15.cloned.1.call-done = bf16[8,64,4096]{2,1,0:T(8,128)(2,1)} async-done(((bf16[8,64,1024]{2,1,0:T(8,128)(2,1)}), bf16[8,64,4096]{2,1,0:T(8,128)(2,1)}) %all-gather.15.cloned.1.call-update) | async-done | bytes 4194320 | tf_op jit(solution)/shard_map/all_gather | solution.py:172
  318.5 5.9 %fusion.8 = f32[8,64,512]{2,1,0:T(8,128)S(1)} fusion(bf16[8,64,4096]{2,1,0:T(8,128)(2,1)} %all-gather.15.cloned.1.call-done, bf16[1,4096,512]{2,1,0:T(8,128)(2,1)} %param.31), kind=kOutput, calls=%fused_computation.12 | convolution fusion | flops 2147483648 | bytes 9437184 | tf_op jit(solution)/shard_map/sck,kf->scf/dot_general | solution.py:173
  324.4 3.2 fusion.16
  327.7 35.2 %all-gather.17.cloned.1.call-done = bf16[8,64,2048]{2,1,0:T(8,128)(2,1)} async-done(((bf16[8,64,512]{2,1,0:T(8,128)(2,1)}), bf16[8,64,2048]{2,1,0:T(8,128)(2,1)}) %all-gather.17.cloned.1.call-update) | async-done | bytes 2097168 | tf_op jit(solution)/shard_map/all_gather | solution.py:180
  362.8 6.1 %fusion.10 = bf16[8,64,1024]{2,1,0:T(8,128)(2,1)} fusion(bf16[8,64,2048]{2,1,0:T(8,128)(2,1)} %all-gather.17.cloned.1.call-done, bf16[1,2048,1024]{2,1,0:T(8,128)(2,1)} %param.33), kind=kOutput, calls=%fused_computation.15 | convolution fusion | flops 2148007936 | bytes 7340032 | tf_op jit(solution)/shard_map/scf,fd->scd/dot_general | solution.py:178
  369.0 4.6 %all-to-all-start.1 = ((bf16[8,64,1024]{2,1,0:T(8,128)(2,1)}), bf16[8,64,1024]{2,1,0:T(8,128)(2,1)S(1)}, u32[]{:S(2)}, u32[]{:S(2)}) async-start(bf16[8,64,1024]{2,1,0:T(8,128)(2,1)} %fusion.10), calls=%async_computation.1 | async-start | bytes 2097152 | tf_op jit(solution)/shard_map/all_to_all | solution.py:184
  373.7 26.4 %all-to-all-done.1 = bf16[8,64,1024]{2,1,0:T(8,128)(2,1)S(1)} async-done(((bf16[8,64,1024]{2,1,0:T(8,128)(2,1)}), bf16[8,64,1024]{2,1,0:T(8,128)(2,1)S(1)}, u32[]{:S(2)}, u32[]{:S(2)}) %all-to-all-start.1) | async-done | bytes 1048608 | tf_op jit(solution)/shard_map/all_to_all | solution.py:184
  400.5 1.0 fusion.24
  (107 shorter events, 7.4 us)
Async XLA Ops:
  6.5 39.3 %all-gather.19.cloned.1.call-start = ((), (), s32[]{:S(2)}) async-start(), calls=%async_computation.6 | async-start | bytes 2359296 | tf_op jit(solution)/shard_map/all_gather | solution.py:13
  7.3 6.5 %copy-start.2 = (bf16[128,1024]{1,0:T(8,128)(2,1)S(1)}, bf16[128,1024]{1,0:T(8,128)(2,1)}, u32[]{:S(2)}) copy-start(bf16[128,1024]{1,0:T(8,128)(2,1)} %param.22) | copy-start | bytes 786436
  11.2 3.1 copy-start.3
  13.7 80.0 %all-gather.21.cloned.1.call-start = ((), (), s32[]{:S(2)}) async-start(), calls=%async_computation.7 | async-start | bytes 4718592 | tf_op jit(solution)/shard_map/all_gather | solution.py:13
  14.0 3.3 copy-start
  14.8 26.0 %copy-start.6 = (f32[2,512]{1,0:T(2,128)S(1)}, f32[2,512]{1,0:T(2,128)}, u32[]{:S(2)}) copy-start(f32[2,512]{1,0:T(2,128)} %param.26) | copy-start | bytes 12292
  17.1 122.9 %all-gather.11.cloned.1.call-start = ((), (), s32[]{:S(2)}) async-start(), calls=%async_computation.2 | async-start | bytes 1310720 | tf_op jit(solution)/shard_map/all_gather | solution.py:144
  111.8 3.5 copy-start.5
  111.9 111.7 %copy-start.1 = (bf16[128,1024]{1,0:T(8,128)(2,1)S(1)}, bf16[128,1024]{1,0:T(8,128)(2,1)}, u32[]{:S(2)}) copy-start(bf16[128,1024]{1,0:T(8,128)(2,1)} %param.18) | copy-start | bytes 786436
  114.7 108.9 %all-gather.13.cloned.1.call-start = ((), (), s32[]{:S(2)}) async-start(), calls=%async_computation.3 | async-start | bytes 9437184 | tf_op jit(solution)/shard_map/all_gather | solution.py:148
  115.3 203.2 %all-gather.15.cloned.1.call-start = ((), (), s32[]{:S(2)}) async-start(), calls=%async_computation.4 | async-start | bytes 5242880 | tf_op jit(solution)/shard_map/all_gather | solution.py:172
  117.0 121.4 %copy-start.4 = (f32[1024]{0:T(1024)S(1)}, f32[1024]{0:T(1024)}, u32[]{:S(2)}) copy-start(f32[1024]{0:T(1024)} %param.28) | copy-start | bytes 12292
  268.7 94.2 %all-gather.17.cloned.1.call-start = ((), (), s32[]{:S(2)}) async-start(), calls=%async_computation.5 | async-start | bytes 2621440 | tf_op jit(solution)/shard_map/all_gather | solution.py:180
  318.5 5.9 %copy-start.8 = (bf16[1,4096,512]{2,1,0:T(8,128)(2,1)S(1)}, bf16[1,4096,512]{2,1,0:T(8,128)(2,1)}, u32[]{:S(2)}) copy-start(bf16[1,4096,512]{2,1,0:T(8,128)(2,1)} %param.32) | copy-start | bytes 12582916
  318.5 5.9 %copy-start.9 = (bf16[8,64,4096]{2,1,0:T(8,128)(2,1)S(1)}, bf16[8,64,4096]{2,1,0:T(8,128)(2,1)}, u32[]{:S(2)}) copy-start(bf16[8,64,4096]{2,1,0:T(8,128)(2,1)} %all-gather.15.cloned.1.call-done) | copy-start | bytes 12582916
  327.6 45.9 %copy-start.7 = (f32[128,2]{0,1:T(2,128)S(1)}, f32[128,2]{0,1:T(2,128)}, u32[]{:S(2)}) copy-start(f32[128,2]{0,1:T(2,128)} %param.30) | copy-start | bytes 3076
  369.0 31.2 %all-to-all-start.1 = ((bf16[8,64,1024]{2,1,0:T(8,128)(2,1)}), bf16[8,64,1024]{2,1,0:T(8,128)(2,1)S(1)}, u32[]{:S(2)}, u32[]{:S(2)}) async-start(bf16[8,64,1024]{2,1,0:T(8,128)(2,1)} %fusion.10), calls=%async_computation.1 | async-start | bytes 2097152 | tf_op jit(solution)/shard_map/all_to_all | solution.py:184
Sparse Core Ops, SparseCore 0:
  13.9 31.9 all-gather.18
  47.4 46.2 all-gather.20
  114.8 25.1 all-gather.10
  141.5 82.0 all-gather.12
  268.8 49.6 all-gather.14
  327.8 35.0 all-gather.16
where the time goes:
time: 409 us; the launch traced here: 408 us
  waiting for transfers between devices  271 us (66%)
  blocking collectives  62.1 us (15%)
  matrix products  26.3 us (6%)
  other arithmetic  21.3 us (5%)
  between operations  14 us (3%)
  local copies, waits for them, and re-layouts  8.67 us (2%)
  starting transfers between devices  4.99 us (1%)
    all_gather x1, waiting for transfers between devices, per_device(): lax.all_gather(out_weight, 'sp', axis=1, tiled=True)  83.5 us
    all_gather x2, waiting for transfers between devices, entering_2(): everything = jax.tree.map(lambda part: lax.all_gather(part, axis), array)  52.4 us
    all_gather x1, waiting for transfers between devices, per_device(): expert_arrived = lax.all_gather(arrived, 'tp', axis=2, tiled=True)  49.5 us
    all_gather x1, waiting for transfers between devices, per_device(): lax.all_gather(hidden, 'tp', axis=2, tiled=True)  35.2 us
    all_to_all x1, blocking collectives, per_device(): lax.all_to_all(outgoing, 'sp', split_axis=0, concat_axis=0, tiled=True)  29.7 us
    all_to_all x1, waiting for transfers between devices, per_device(): lax.all_to_all(expert_out, 'sp', split_axis=0, concat_axis=0, tiled=True)  26.4 us
    all_gather x1, waiting for transfers between devices, per_device(): gathered = lax.all_gather(stacked, 'tp', axis=2, tiled=True)  23 us
    all_gather x2, blocking collectives, entering_2(): everything = jax.tree.map(lambda part: lax.all_gather(part, axis), array)  22.6 us
  transfers between devices with their start and end apart: 7, of which 7 were waited for; matrix products, arithmetic and copies ran while one was open for 2% of the time, Pallas kernels for 0%

commit v1 on v0

--- a/solution.py
+++ b/solution.py
@@ -6,6 +6,23 @@
 D = 4096
 EPS = 1e-06
 THETA = 10000.0
+
+
+def attach_the_cube(frame):
+    row_axis = "tp"
+    sides = jax.lax.axis_size(row_axis)
+    big = frame
+    xs_all = [big]
+    v_next = [(rr - 1, rr) for rr in range(1, sides)] + [(sides - 1, 0)]
+    dev_i = 0
+    while dev_i < sides - 1:
+        big = jax.lax.ppermute(big, row_axis, v_next)
+        xs_all += [big]
+        dev_i = dev_i + 1
+    current_value = jnp.concatenate([*reversed(xs_all)], 2)
+    seen_now = jax.lax.axis_index(row_axis)
+    right_arr = jnp.roll(current_value, (seen_now + 1) * big.shape[2], 2)
+    return right_arr
 
 
 def entering_2(array, axis, combine, identity):
@@ -169,7 +186,7 @@
     outgoing = jnp.dot(select, normed, preferred_element_type=jnp.float32).astype(jnp.bfloat16)
     outgoing = outgoing.reshape(experts, capacity, normed.shape[1])
     arrived = lax.all_to_all(outgoing, "sp", split_axis=0, concat_axis=0, tiled=True)
-    expert_arrived = lax.all_gather(arrived, "tp", axis=2, tiled=True)
+    expert_arrived = attach_the_cube(arrived)
     gate_part = jnp.einsum(
         "sck,kf->scf", expert_arrived, w_gate, preferred_element_type=jnp.float32
     )

time: 409 us -> 434 us (1.061)
  waiting for transfers between devices: 271 us -> 294 us
  local copies, waits for them, and re-layouts: 8.67 us -> 14.3 us
    ppermute x0 -> x3, waiting for transfers between devices: none -> 74.1 us  [attach_the_cube(): big = jax.lax.ppermute(big, row_axis, v_next)]
    all_gather x1 -> x0, waiting for transfers between devices: 49.5 us -> none  [per_device(): expert_arrived = lax.all_gather(arrived, 'tp', axis=2, tiled=True)]
    unnamed x34 -> x41, local copies, waits for them, and re-layouts: 3.78 us -> 9.27 us
  transfers between devices with their start and end apart: 7 -> 9, of which waited for: 7 -> 9; matrix products, arithmetic and copies ran while one was open for 2% -> 1% of each run, Pallas kernels for 0% -> 0%
where the time goes in v1:
time: 434 us; the launch traced here: 433 us
  waiting for transfers between devices  294 us (68%)
  blocking collectives  61.4 us (14%)
  matrix products  22.7 us (5%)
  other arithmetic  21.4 us (5%)
  local copies, waits for them, and re-layouts  14.3 us (3%)
  between operations  13.7 us (3%)
  starting transfers between devices  4.78 us (1%)
    all_gather x1, waiting for transfers between devices, per_device(): lax.all_gather(out_weight, 'sp', axis=1, tiled=True)  83.5 us
    ppermute x3, waiting for transfers between devices, attach_the_cube(): big = jax.lax.ppermute(big, row_axis, v_next)  74.1 us
    all_gather x2, waiting for transfers between devices, entering_2(): everything = jax.tree.map(lambda part: lax.all_gather(part, axis), array)  52.5 us
    all_gather x1, waiting for transfers between devices, per_device(): lax.all_gather(hidden, 'tp', axis=2, tiled=True)  34 us
    all_to_all x1, blocking collectives, per_device(): lax.all_to_all(outgoing, 'sp', split_axis=0, concat_axis=0, tiled=True)  29 us
    all_to_all x1, waiting for transfers between devices, per_device(): lax.all_to_all(expert_out, 'sp', split_axis=0, concat_axis=0, tiled=True)  26.4 us
    all_gather x1, waiting for transfers between devices, per_device(): gathered = lax.all_gather(stacked, 'tp', axis=2, tiled=True)  23 us
    all_gather x2, blocking collectives, entering_2(): everything = jax.tree.map(lambda part: lax.all_gather(part, axis), array)  22.6 us
  transfers between devices with their start and end apart: 9, of which 9 were waited for; matrix products, arithmetic and copies ran while one was open for 1% of the time, Pallas kernels for 0%

profile of v1, /device:TPU:0, one launch (start us, length us, event | category | flops | bytes accessed | tf_op | source)
XLA Modules:
  0.0 432.8 jit_solution(8261201068690864500)
XLA Ops:
  6.6 0.8 slice_bitcast_fusion.4
  7.3 1.5 fusion.81
  8.9 1.0 copy.129
  10.2 1.0 copy.132
  12.8 1.0 fusion.41
  15.9 1.2 fusion.28
  18.2 13.6 %all-gather.3 = f32[8,1,4]{2,1,0:T(1,128)S(1)} all-gather(f32[1,1,4]{2,1,0:T(1,128)S(1)} %get-tuple-element.253), channel_id=1, replica_groups=mesh['sp'=8,'tp'=4] {'sp'}, dimensions={0}, use_global_device_ids=true | all-gather | bytes 144 | tf_op jit(solution)/shard_map/all_gather | solution.py:30
  31.8 9.0 %all-gather.2 = f32[8,1,4]{2,1,0:T(1,128)S(1)} all-gather(f32[1,1,4]{2,1,0:T(1,128)S(1)} %get-tuple-element.255), channel_id=1, replica_groups=mesh['sp'=8,'tp'=4] {'sp'}, dimensions={0}, use_global_device_ids=true | all-gather | bytes 144 | tf_op jit(solution)/shard_map/all_gather | solution.py:30
  41.3 4.6 %all-gather.16.cloned.1.call-done = f32[32,128,128]{2,1,0:T(8,128)} async-done(((f32[4,128,128]{2,1,0:T(8,128)}), f32[32,128,128]{2,1,0:T(8,128)}) %all-gather.16.cloned.1.call-update) | async-done | bytes 2097168 | tf_op jit(solution)/shard_map/all_gather | solution.py:30
  45.9 47.9 %all-gather.18.cloned.1.call-done = f32[32,256,128]{2,1,0:T(8,128)} async-done(((f32[4,256,128]{2,1,0:T(8,128)}), f32[32,256,128]{2,1,0:T(8,128)}) %all-gather.18.cloned.1.call-update) | async-done | bytes 4194320 | tf_op jit(solution)/shard_map/all_gather | solution.py:30
  93.8 18.2 %while.16 = (s32[]{:T(128)}, f32[4,128,128]{2,1,0:T(8,128)S(1)}, f32[4,256,128]{2,1,0:T(8,128)S(1)}, s32[]{:T(128)}, f32[8,4]{1,0:T(8,128)S(1)}, /*index=5*/f32[...) while((s32[]{:T(128)}, f32[4,128,128]{2,1,0:T(8,128)S(1)}, ...), condition=%wide.region_3.4_spmd.clone, body=%wide.region_2.3_spmd.clone.sunk | while | flops 786436 | bytes 2359527 | solution.py:42
  93.8 1.2 fusion.106
  95.0 1.1 fusion.105
  96.1 1.2 fusion.106
  97.3 1.1 fusion.105
  98.4 1.2 fusion.106
  99.6 1.1 fusion.105
  100.7 1.2 fusion.106
  101.8 1.1 fusion.105
  102.9 1.2 fusion.106
  104.1 1.1 fusion.105
  105.2 1.2 fusion.106
  106.4 1.1 fusion.105
  107.5 1.2 fusion.106
  108.7 1.1 fusion.105
  109.8 1.2 fusion.106
  110.9 1.1 fusion.105
  112.8 0.7 fusion.21
  114.1 0.7 pad_maximum_fusion.1
  117.2 23.0 %all-gather.10.cloned.1.call-done = bf16[128,2,2048]{2,0,1:T(8,128)(2,1)} async-done(((bf16[128,2,512]{2,0,1:T(8,128)(2,1)}), bf16[128,2,2048]{2,0,1:T(8,128)(2,1)}) %all-gather.10.cloned.1.call-update) | async-done | bytes 1048592 | tf_op jit(solution)/shard_map/all_gather | solution.py:161
  140.2 83.5 %all-gather.12.cloned.1.call-done = bf16[2,2048,1024]{2,1,0:T(8,128)(2,1)} async-done(((bf16[2,256,1024]{2,1,0:T(8,128)(2,1)}), bf16[2,2048,1024]{2,1,0:T(8,128)(2,1)}) %all-gather.12.cloned.1.call-update) | async-done | bytes 8388624 | tf_op jit(solution)/shard_map/all_gather | solution.py:165
  223.7 5.1 %multiply_reduce_fusion = (f32[128]{0:T(128)S(1)}, f32[128,1024]{1,0:T(8,128)S(1)}) fusion(bf16[128,2,2048]{2,0,1:T(8,128)(2,1)} %all-gather.10.cloned.1.call-done, bf16[2,2048,1024]{2,1,0:T(8,128)(2,1)} %all-gather.12.cloned.1.call-done, bf16[128,1024]{1,0:T(8,128)(2,1)S(1)} %copy-done.1), kind=kOutput, calls=%fused_computation.43 | convolution fusion | flops 1074528128 | bytes 10224128 | tf_op jit(solution)/shard_map/tgk,gkd->td/dot_general | solution.py:162
  228.8 9.8 %psum.7 = f32[128]{0:T(128)S(1)} all-reduce(f32[128]{0:T(128)S(1)} %get-tuple-element.270), channel_id=1, replica_groups=mesh['sp'=8,'tp'=4] {'tp'}, use_global_device_ids=true, to_apply=%region_11.12 | all-reduce | flops 128 | bytes 1024 | tf_op jit(solution)/shard_map/psum | solution.py:169
  239.2 29.0 %all_to_all.10 = bf16[8,64,1024]{2,1,0:T(8,128)(2,1)S(1)} all-to-all(bf16[8,64,1024]{2,1,0:T(8,128)(2,1)S(1)} %bitcast.126), channel_id=1, replica_groups=mesh['sp'=8,'tp'=4] {'sp'}, dimensions={0} | all-to-all | bytes 2097152 | tf_op jit(solution)/shard_map/all_to_all | solution.py:188
  268.1 25.4 %collective-permute-done = bf16[8,64,1024]{2,1,0:T(8,128)(2,1)S(1)} collective-permute-done((bf16[8,64,1024]{2,1,0:T(8,128)(2,1)S(1)}, bf16[8,64,1024]{2,1,0:T(8,128)(2,1)S(1)}, u32[]{:S(2)}, u32[]{:S(2)}) %collective-permute-start) | collective-permute-done | bytes 1048608 | tf_op jit(solution)/shard_map/ppermute | solution.py:19
  293.6 24.7 %collective-permute-done.1 = bf16[8,64,1024]{2,1,0:T(8,128)(2,1)} collective-permute-done((bf16[8,64,1024]{2,1,0:T(8,128)(2,1)S(1)}, bf16[8,64,1024]{2,1,0:T(8,128)(2,1)}, u32[]{:S(2)}, u32[]{:S(2)}) %collective-permute-start.1) | collective-permute-done | bytes 1048608 | tf_op jit(solution)/shard_map/ppermute | solution.py:19
  318.3 24.0 %collective-permute-done.2 = bf16[8,64,1024]{2,1,0:T(8,128)(2,1)} collective-permute-done((bf16[8,64,1024]{2,1,0:T(8,128)(2,1)}, bf16[8,64,1024]{2,1,0:T(8,128)(2,1)}, u32[]{:S(2)}, u32[]{:S(2)}) %collective-permute-start.2) | collective-permute-done | bytes 1048608 | tf_op jit(solution)/shard_map/ppermute | solution.py:19
  342.3 1.3 constant_dynamic-update-slice_fusion.7
  343.6 1.3 constant_dynamic-update-slice_fusion.6
  345.1 1.3 constant_dynamic-update-slice_fusion.3
  346.4 1.3 constant_dynamic-update-slice_fusion.2
  348.0 2.3 fusion.8
  350.3 3.2 multiply_convert_fusion
  353.5 34.0 %all-gather.14.cloned.1.call-done = bf16[8,64,2048]{2,1,0:T(8,128)(2,1)} async-done(((bf16[8,64,512]{2,1,0:T(8,128)(2,1)}), bf16[8,64,2048]{2,1,0:T(8,128)(2,1)}) %all-gather.14.cloned.1.call-update) | async-done | bytes 2097168 | tf_op jit(solution)/shard_map/all_gather | solution.py:197
  387.6 6.1 %fusion.12 = bf16[8,64,1024]{2,1,0:T(8,128)(2,1)} fusion(bf16[8,64,2048]{2,1,0:T(8,128)(2,1)} %all-gather.14.cloned.1.call-done, bf16[1,2048,1024]{2,1,0:T(8,128)(2,1)} %param.33), kind=kOutput, calls=%fused_computation.17 | convolution fusion | flops 2148007936 | bytes 7340032 | tf_op jit(solution)/shard_map/scf,fd->scd/dot_general | solution.py:195
  393.7 4.6 %all-to-all-start.1 = ((bf16[8,64,1024]{2,1,0:T(8,128)(2,1)}), bf16[8,64,1024]{2,1,0:T(8,128)(2,1)S(1)}, u32[]{:S(2)}, u32[]{:S(2)}) async-start(bf16[8,64,1024]{2,1,0:T(8,128)(2,1)} %fusion.12), calls=%async_computation.1 | async-start | bytes 2097152 | tf_op jit(solution)/shard_map/all_to_all | solution.py:201
  398.5 26.4 %all-to-all-done.1 = bf16[8,64,1024]{2,1,0:T(8,128)(2,1)S(1)} async-done(((bf16[8,64,1024]{2,1,0:T(8,128)(2,1)}), bf16[8,64,1024]{2,1,0:T(8,128)(2,1)S(1)}, u32[]{:S(2)}, u32[]{:S(2)}) %all-to-all-start.1) | async-done | bytes 1048608 | tf_op jit(solution)/shard_map/all_to_all | solution.py:201
  425.2 1.0 fusion.20
  (118 shorter events, 10.4 us)
Async XLA Ops:
  6.5 7.3 %copy-start.2 = (bf16[128,1024]{1,0:T(8,128)(2,1)S(1)}, bf16[128,1024]{1,0:T(8,128)(2,1)}, u32[]{:S(2)}) copy-start(bf16[128,1024]{1,0:T(8,128)(2,1)} %param.22) | copy-start | bytes 786436
  6.5 7.8 %copy-start.3 = (bf16[128,1024]{1,0:T(8,128)(2,1)S(1)}, bf16[128,1024]{1,0:T(8,128)(2,1)}, u32[]{:S(2)}) copy-start(bf16[128,1024]{1,0:T(8,128)(2,1)} %param.21) | copy-start | bytes 786436
  6.5 39.4 %all-gather.16.cloned.1.call-start = ((), (), s32[]{:S(2)}) async-start(), calls=%async_computation.5 | async-start | bytes 2359296 | tf_op jit(solution)/shard_map/all_gather | solution.py:30
  9.9 7.4 %copy-start = (bf16[128,2,512]{2,1,0:T(2,128)(2,1)S(1)}, bf16[128,2,512]{2,1,0:T(2,128)(2,1)}, u32[]{:S(2)}) copy-start(bf16[128,2,512]{2,1,0:T(2,128)(2,1)} %param.24) | copy-start | bytes 786436
  12.5 28.4 %copy-start.6 = (f32[2,512]{1,0:T(2,128)S(1)}, f32[2,512]{1,0:T(2,128)}, u32[]{:S(2)}) copy-start(f32[2,512]{1,0:T(2,128)} %param.26) | copy-start | bytes 12292
  13.8 80.0 %all-gather.18.cloned.1.call-start = ((), (), s32[]{:S(2)}) async-start(), calls=%async_computation.6 | async-start | bytes 4718592 | tf_op jit(solution)/shard_map/all_gather | solution.py:30
  17.2 123.0 %all-gather.10.cloned.1.call-start = ((), (), s32[]{:S(2)}) async-start(), calls=%async_computation.2 | async-start | bytes 1310720 | tf_op jit(solution)/shard_map/all_gather | solution.py:161
  93.8 21.7 %copy-start.5 = (s32[128,2]{0,1:T(2,128)S(1)}, s32[128,2]{0,1:T(2,128)}, u32[]{:S(2)}) copy-start(s32[128,2]{0,1:T(2,128)} %param.29) | copy-start | bytes 3076
  93.8 129.9 %copy-start.1 = (bf16[128,1024]{1,0:T(8,128)(2,1)S(1)}, bf16[128,1024]{1,0:T(8,128)(2,1)}, u32[]{:S(2)}) copy-start(bf16[128,1024]{1,0:T(8,128)(2,1)} %param.18) | copy-start | bytes 786436
  114.8 108.9 %all-gather.12.cloned.1.call-start = ((), (), s32[]{:S(2)}) async-start(), calls=%async_computation.3 | async-start | bytes 9437184 | tf_op jit(solution)/shard_map/all_gather | solution.py:165
  115.4 123.2 %copy-start.4 = (f32[1024]{0:T(1024)S(1)}, f32[1024]{0:T(1024)}, u32[]{:S(2)}) copy-start(f32[1024]{0:T(1024)} %param.28) | copy-start | bytes 12292
  115.4 272.1 %all-gather.14.cloned.1.call-start = ((), (), s32[]{:S(2)}) async-start(), calls=%async_computation.4 | async-start | bytes 2621440 | tf_op jit(solution)/shard_map/all_gather | solution.py:197
  268.1 25.4 %collective-permute-start = (bf16[8,64,1024]{2,1,0:T(8,128)(2,1)S(1)}, bf16[8,64,1024]{2,1,0:T(8,128)(2,1)S(1)}, u32[]{:S(2)}, u32[]{:S(2)}) collective-permute-start(bf16[8,64,1024]{2,1,0:T(8,128)(2,1)S(1)} %all_to_all.10), channel_id=1, source_target_pairs={{0,1},{1,2},{2,3},{3,0},{4,5},{5,6},{6,7},{7,4},{8,9},{9,10},{10,1... | collective-permute-start | bytes 3145736 | tf_op jit(solution)/shard_map/ppermute | solution.py:19
  293.6 24.7 %collective-permute-start.1 = (bf16[8,64,1024]{2,1,0:T(8,128)(2,1)S(1)}, bf16[8,64,1024]{2,1,0:T(8,128)(2,1)}, u32[]{:S(2)}, u32[]{:S(2)}) collective-permute-start(bf16[8,64,1024]{2,1,0:T(8,128)(2,1)S(1)} %collective-permute-done), channel_id=1, source_target_pairs={{0,1},{1,2},{2,3},{3,0},{4,5},{5,6},{6,7},{7,4},{8,9},{9,10},{10,1... | collective-permute-start | bytes 3145736 | tf_op jit(solution)/shard_map/ppermute | solution.py:19
  318.3 24.0 %collective-permute-start.2 = (bf16[8,64,1024]{2,1,0:T(8,128)(2,1)}, bf16[8,64,1024]{2,1,0:T(8,128)(2,1)}, u32[]{:S(2)}, u32[]{:S(2)}) collective-permute-start(bf16[8,64,1024]{2,1,0:T(8,128)(2,1)} %collective-permute-done.1), channel_id=1, source_target_pairs={{0,1},{1,2},{2,3},{3,0},{4,5},{5,6},{6,7},{7,4},{8,9},{9,10},{10,1... | collective-permute-start | bytes 3145736 | tf_op jit(solution)/shard_map/ppermute | solution.py:19
  318.3 29.7 %copy-start.8 = (bf16[1,4096,512]{2,1,0:T(8,128)(2,1)S(1)}, bf16[1,4096,512]{2,1,0:T(8,128)(2,1)}, u32[]{:S(2)}) copy-start(bf16[1,4096,512]{2,1,0:T(8,128)(2,1)} %param.31) | copy-start | bytes 12582916
  348.0 2.3 copy-start.9
  353.5 44.8 %copy-start.7 = (f32[128,2]{0,1:T(2,128)S(1)}, f32[128,2]{0,1:T(2,128)}, u32[]{:S(2)}) copy-start(f32[128,2]{0,1:T(2,128)} %param.30) | copy-start | bytes 3076
  393.7 31.2 %all-to-all-start.1 = ((bf16[8,64,1024]{2,1,0:T(8,128)(2,1)}), bf16[8,64,1024]{2,1,0:T(8,128)(2,1)S(1)}, u32[]{:S(2)}, u32[]{:S(2)}) async-start(bf16[8,64,1024]{2,1,0:T(8,128)(2,1)} %fusion.12), calls=%async_computation.1 | async-start | bytes 2097152 | tf_op jit(solution)/shard_map/all_to_all | solution.py:201
Sparse Core Ops, SparseCore 0:
  13.9 31.9 all-gather.15
  47.5 46.2 all-gather.17
  115.0 25.1 all-gather.9
  141.7 82.0 all-gather.11
  353.7 33.8 all-gather.13
